TPU v7x, 512 devices: a whole 4x4x16 slice. The times are simulated.
512 devices in a mesh: ep: 128 (over z, x, core), tp: 4 (over y).
Axes of the slice: x: 4, y: 4, z: 16, core: 2. Of those that a mesh axis runs over, the one named last changes fastest.
Arguments:
- tokens: bfloat16 [1024, 1024], P('ep'), may hold values from -6 to 6
- lengths: int32 [1024], P('ep'), may hold values from 1 to 512, as said below
- cache_keys: bfloat16 [1024, 512, 4, 128], P('ep', None, 'tp'), may hold values from -2.5 to 2.5
- cache_values: bfloat16 [1024, 512, 4, 128], P('ep', None, 'tp'), may hold values from -6 to 6
- cache_cum: float32 [1024, 4, 512], P('ep', 'tp'), may hold values from -1536 to 0, as said below
- norm_gain: bfloat16 [1024], replicated, may hold values from 0.099609375 to 1.8984375
- query_weight: bfloat16 [1024, 1024], P(None, 'tp'), may hold values from -0.1875 to 0.1875
- key_weight: bfloat16 [1024, 512], P(None, 'tp'), may hold values from -0.1875 to 0.1875
- value_weight: bfloat16 [1024, 512], P(None, 'tp'), may hold values from -0.1875 to 0.1875
- forget_weight: bfloat16 [1024, 4], P(None, 'tp'), may hold values from -0.1875 to 0.1875
- forget_bias: float32 [4], P('tp'), may hold values from -1 to 2
- query_gain: bfloat16 [128], replicated, may hold values from 0.29882812 to 2.5
- key_gain: bfloat16 [128], replicated, may hold values from 0.099609375 to 1.8984375
- out_weight: bfloat16 [1024, 1024], P('tp'), may hold values from -0.1875 to 0.1875
- ffn_gain: bfloat16 [1024], replicated, may hold values from 0.099609375 to 1.8984375
- mix_weight: bfloat16 [1024], replicated, may hold values from -0.1875 to 0.1875
- shared_gate: bfloat16 [1024, 4096], P(None, 'ep'), may hold values from -0.1875 to 0.1875
- shared_up: bfloat16 [1024, 4096], P(None, 'ep'), may hold values from -0.1875 to 0.1875
- shared_down: bfloat16 [4096, 1024], P('ep', 'tp'), may hold values from -0.09375 to 0.09375
- routes: int32 [1024, 2], P('ep'), may hold values from 0 to 127, all different within a row; in each aligned block of 8 rows (0 to 7, 8 to 15, ...) at most 4 rows name the same one
- route_weights: float32 [1024, 2], P('ep'), may hold values from 0.1 to 1
- expert_gate: bfloat16 [128, 1024, 512], P('ep', None, 'tp'), may hold values from -0.1875 to 0.1875
- expert_up: bfloat16 [128, 1024, 512], P('ep', None, 'tp'), may hold values from -0.1875 to 0.1875
- expert_down: bfloat16 [128, 512, 1024], P('ep', 'tp'), may hold values from -0.25 to 0.25
Outputs:
- layer_out: bfloat16 [1024, 1024], P('ep', 'tp')
Inputs may be any that keep to these rules, and one draw needn't show every extreme that they name: `lengths`: at least one sequence has exactly 512 cached positions. `cache_cum`: along the positions each row never rises. `routes`: the 2 experts of a token differ; among the 8 rows of one device no expert is named by more than 4 rows, a bound that some block reaches.
All inputs are finite; a program needn't handle non-finite values.
Results may differ from a plain program's by a relative error of at most 0.013.
Values may be sent and summed in bfloat16 or wider, within the bound.
A program may use at most 64 MiB of HBM per device.

v0:
```python
import jax
import jax.numpy as jnp
from jax import lax
from jax.sharding import Mesh
from jax.sharding import PartitionSpec as P

CAP = 4
EP = ("ep_0", "ep_1", "ep_2")


epsilon = 1e-06


def copy_for_each(shard, axis):
    peers = lax.axis_size(axis)
    return lax.all_to_all(
        jnp.broadcast_to(shard[None], (peers, *shard.shape)), axis, 0, 0, tiled=True
    )


def of_everyone(shard, axis):
    return copy_for_each(shard, axis).astype(jnp.float32).sum(axis=0)


def cut_along(shard, dim, peers):
    before, after = (shard.shape[:dim], shard.shape[dim + 1 :])
    return jnp.moveaxis(shard.reshape(*before, peers, -1, *after), dim, 0)


def summed_on_arrival(shard, axis, dim):
    peers = lax.axis_size(axis)
    tiles = lax.all_to_all(cut_along(shard, dim, peers), axis, 0, 0, tiled=True)
    return jnp.sum(tiles.astype(jnp.float32), axis=0)


def sum_in_order(tiles, axes, sequence):
    shape = [lax.axis_size(a) for a in axes]
    tiles = tiles.reshape(*shape, *tiles.shape[1:])
    tiles = tiles.transpose(*sequence, *range(len(axes), tiles.ndim))
    tiles = tiles.reshape(-1, *tiles.shape[len(axes) :])
    for k in sequence:
        tiles = lax.psum_scatter(tiles, axes[k], scatter_dimension=0, tiled=True)
    return tiles[0]


def summed_rows(shard, axes, sequence, dim):
    peers = lax.axis_size(axes)
    return sum_in_order(cut_along(shard, dim, peers), axes, sequence)


def rms_norm(values, gain):
    values = values.astype(jnp.float32)
    return (
        values
        * lax.rsqrt(jnp.mean(values * values, axis=-1, keepdims=True) + epsilon)
        * gain.astype(jnp.float32)
    )


def per_device(
    tokens,
    lengths,
    cache_keys,
    cache_values,
    cache_cum,
    norm_gain,
    query_weight,
    key_weight,
    value_weight,
    forget_weight,
    forget_bias,
    query_gain,
    key_gain,
    out_weight,
    ffn_gain,
    mix_weight,
    shared_gate,
    shared_up,
    shared_down,
    routes,
    route_weights,
    expert_gate,
    expert_up,
    expert_down,
):
    seq_rows = tokens.shape[0]
    cache_len = cache_keys.shape[1]
    kv_local = cache_keys.shape[2]
    head_size = cache_keys.shape[3]
    normed = rms_norm(tokens, norm_gain).astype(jnp.bfloat16)
    query = jnp.dot(normed, query_weight, preferred_element_type=jnp.float32)
    query = rms_norm(query.reshape(seq_rows, kv_local, -1, head_size), query_gain).astype(
        jnp.bfloat16
    )
    new_key = jnp.dot(normed, key_weight, preferred_element_type=jnp.float32)
    new_key = rms_norm(new_key.reshape(seq_rows, kv_local, head_size), key_gain).astype(
        jnp.bfloat16
    )
    new_value = jnp.dot(normed, value_weight, preferred_element_type=jnp.float32).astype(
        jnp.bfloat16
    )
    new_value = new_value.reshape(seq_rows, kv_local, head_size)
    new_log = jax.nn.log_sigmoid(
        jnp.dot(normed, forget_weight, preferred_element_type=jnp.float32) + forget_bias
    )
    position = jnp.arange(cache_len, dtype=jnp.int32)
    live = position[None, :] < lengths[:, None]
    at_last = (position[None, :] == lengths[:, None] - 1)[:, None, :]
    last_cum = jnp.sum(jnp.where(at_last, cache_cum, 0.0), axis=-1)
    gate_bias = last_cum[:, :, None] - cache_cum + new_log[:, :, None]
    score_scale = head_size ** (-0.5)
    past = (
        jnp.einsum("skgd,spkd->skgp", query, cache_keys, preferred_element_type=jnp.float32)
        * score_scale
    )
    past = past + gate_bias[:, :, None, :]
    past = jnp.where(live[:, None, None, :], past, -jnp.inf)
    own = (
        jnp.sum(query.astype(jnp.float32) * new_key.astype(jnp.float32)[:, :, None, :], axis=-1)
        * score_scale
    )
    past_exp = jnp.exp(past)
    own_exp = jnp.exp(own)
    denominator = jnp.sum(past_exp, axis=-1) + own_exp
    past_prob = (past_exp / denominator[..., None]).astype(jnp.bfloat16)
    own_prob = (own_exp / denominator).astype(jnp.bfloat16)
    mixed = jnp.einsum(
        "skgp,spkd->skgd", past_prob, cache_values, preferred_element_type=jnp.float32
    )
    mixed = (
        mixed
        + own_prob.astype(jnp.float32)[..., None] * new_value.astype(jnp.float32)[:, :, None, :]
    )
    heads_out = mixed.astype(jnp.bfloat16).reshape(seq_rows, -1)
    partial_value = jnp.dot(heads_out, out_weight, preferred_element_type=jnp.float32)
    attended = of_everyone(partial_value.astype(jnp.bfloat16), "tp").astype(jnp.float32)
    residual = tokens.astype(jnp.float32) + attended
    ffn_in = rms_norm(residual, ffn_gain).astype(jnp.bfloat16)
    mix_gate = jax.nn.sigmoid(jnp.dot(ffn_in, mix_weight, preferred_element_type=jnp.float32))
    slice_width = ffn_in.shape[1] // lax.axis_size("tp")
    slice_start = lax.axis_index("tp") * slice_width
    ep_count = lax.axis_size(EP)
    local_experts = expert_gate.shape[0]
    num_experts = ep_count * local_experts
    topk = routes.shape[1]
    n_assign = seq_rows * topk
    order = jnp.arange(n_assign, dtype=jnp.int32)
    earlier = order[None, :] < order[:, None]
    slot_ids = jnp.arange(num_experts * CAP, dtype=jnp.int32)
    flat_route = routes.reshape(-1)
    same_expert = flat_route[:, None] == flat_route[None, :]
    slot_rank = jnp.sum(jnp.logical_and(same_expert, earlier), axis=1)
    slot_index = flat_route * CAP + slot_rank
    gathered_rows, gathered_routes = (
        lax.all_gather(ffn_in, EP, axis=0, tiled=True),
        lax.all_gather(routes, EP, axis=0, tiled=True),
    )
    pre_gate = jnp.dot(gathered_rows, shared_gate, preferred_element_type=jnp.float32)
    pre_up = jnp.dot(gathered_rows, shared_up, preferred_element_type=jnp.float32)
    shared_hidden = (jax.nn.silu(pre_gate) * pre_up).astype(jnp.bfloat16)
    terms = jnp.dot(shared_hidden, shared_down, preferred_element_type=jnp.float32)
    block_routes = gathered_routes.reshape(ep_count, n_assign)
    local_id = block_routes - lax.axis_index(EP) * local_experts
    mine = jnp.logical_and(local_id >= 0, local_id < local_experts)
    same_block = block_routes[:, :, None] == block_routes[:, None, :]
    block_rank = jnp.sum(jnp.logical_and(same_block, earlier[None, :, :]), axis=2)
    source = jnp.arange(ep_count, dtype=jnp.int32)[:, None]
    own_slot = source * (local_experts * CAP) + local_id * CAP + block_rank
    own_slot = jnp.where(mine, own_slot, -1).reshape(-1)
    pick_table = (own_slot[None, :] == slot_ids[:, None]).astype(jnp.bfloat16)
    repeated_all = jnp.repeat(gathered_rows, topk, axis=0)
    received = jnp.dot(pick_table, repeated_all, preferred_element_type=jnp.float32).astype(
        jnp.bfloat16
    )
    received = received.reshape(ep_count, local_experts, CAP, ffn_in.shape[1])
    pre_gate = jnp.einsum(
        "nekd,edf->nekf", received, expert_gate, preferred_element_type=jnp.float32
    )
    pre_up = jnp.einsum("nekd,edf->nekf", received, expert_up, preferred_element_type=jnp.float32)
    hidden = (jax.nn.silu(pre_gate) * pre_up).astype(jnp.bfloat16)
    part_out = jnp.einsum("nekf,efd->nekd", hidden, expert_down, preferred_element_type=jnp.float32)
    summed = summed_on_arrival(part_out.astype(jnp.bfloat16), "tp", 3)
    results = summed.astype(jnp.bfloat16)
    dense = summed_rows(terms, EP, (2, 0, 1), 0)
    returned = lax.all_to_all(results, EP, split_axis=0, concat_axis=0, tiled=True)
    returned = returned.reshape(num_experts * CAP, -1).astype(jnp.float32)
    norm_weights = route_weights / jnp.sum(route_weights, axis=1, keepdims=True)
    slot_table = slot_index.reshape(seq_rows, topk)
    combine = jnp.sum(
        (slot_table[:, :, None] == slot_ids[None, None, :]) * norm_weights[:, :, None], axis=1
    )
    routed = jnp.dot(combine, returned, precision=lax.Precision.HIGHEST)
    residual_slice = lax.dynamic_slice_in_dim(residual, slice_start, slice_width, 1)
    return (residual_slice + mix_gate[:, None] * dense + routed).astype(jnp.bfloat16)


def solution(mesh):
    finer = Mesh(mesh.devices.reshape(16, 4, 2, mesh.shape["tp"]), ("ep_0", "ep_1", "ep_2", "tp"))
    placed = (
        P(EP, None),
        P(EP),
        P(EP, None, "tp", None),
        P(EP, None, "tp", None),
        P(EP, "tp", None),
        P(),
        P(None, "tp"),
        P(None, "tp"),
        P(None, "tp"),
        P(None, "tp"),
        P("tp"),
        P(),
        P(),
        P("tp", None),
        P(),
        P(),
        P(None, EP),
        P(None, EP),
        P(EP, "tp"),
        P(EP, None),
        P(EP, None),
        P(EP, None, "tp"),
        P(EP, None, "tp"),
        P(EP, "tp", None),
    )
    return jax.shard_map(
        per_device, mesh=finer, in_specs=placed, out_specs=P(EP, "tp"), check_vma=False
    )
```

profile of v0, /device:TPU:1, one launch (start us, length us, event | category | flops | bytes accessed | tf_op | source)
XLA Modules:
  0.0 318.6 jit_solution(15933887718298431837)
XLA Ops:
  6.5 0.8 broadcast_add_fusion
  7.3 0.7 iota_compare_fusion.5
  8.7 0.7 convert_element_type.133
  9.4 0.7 convert_element_type.137
  10.0 0.8 fusion.43
  10.9 0.7 convert_element_type.131
  11.6 1.2 fusion.14
  12.7 1.3 multiply_reduce_fusion.2
  14.1 1.3 fusion.49
  15.6 0.2 multiply_reduce_fusion.1
  15.8 0.9 fusion.47
  16.8 0.9 fusion.62
  17.7 0.8 subtract_add_fusion
  18.6 0.5 fusion.71
  19.1 0.3 fusion.13
  19.4 0.2 convolution_convert_fusion.1
  19.6 0.6 broadcast_in_dim.26
  20.2 5.0 %all-to-all-start = ((bf16[4,8,1024]{2,1,0:T(8,128)(2,1)}), bf16[4,8,1024]{2,1,0:T(8,128)(2,1)S(1)}, u32[]{:S(2)}, u32[]{:S(2)}) async-start(bf16[4,8,1024]{2,1,0:T(8,128)(2,1)} %broadcast_in_dim.26), calls=%async_computation | async-start | bytes 131072 | tf_op jit(solution)/shard_map/all_to_all | solution.py:16
  25.2 4.5 %all-to-all-done = bf16[4,8,1024]{2,1,0:T(8,128)(2,1)S(1)} async-done(((bf16[4,8,1024]{2,1,0:T(8,128)(2,1)}), bf16[4,8,1024]{2,1,0:T(8,128)(2,1)S(1)}, u32[]{:S(2)}, u32[]{:S(2)}) %all-to-all-start) | async-done | bytes 65568 | tf_op jit(solution)/shard_map/all_to_all | solution.py:16
  29.9 0.7 multiply_convert_fusion
  30.6 91.3 %all-gather = s32[128,8,2]{1,2,0:T(2,128)S(1)} all-gather(s32[1,8,2]{1,2,0:T(2,128)S(1)} %bitcast.132), channel_id=1, replica_groups=mesh['ep_0'=16,'ep_1'=4,'ep_2'=2,'tp'=4] {'ep_0','ep_1','ep_2'}, dimensions={0}, use_global_device_ids=true | all-gather | bytes 8256 | tf_op jit(solution)/shard_map/all_gather | solution.py:156
  122.1 0.1 convert_reduce_fusion
  122.2 53.6 %all-gather.3.cloned.1.call-done = bf16[1024,1024]{1,0:T(8,128)(2,1)} async-done(((bf16[8,1024]{1,0:T(8,128)(2,1)}), bf16[1024,1024]{1,0:T(8,128)(2,1)}) %all-gather.3.cloned.1.call-update) | async-done | bytes 2097168 | tf_op jit(solution)/shard_map/all_gather | solution.py:155
  175.8 2.5 fusion.72
  178.3 2.0 fusion.7
  180.3 2.4 copy.100
  183.2 0.3 copy.105
  183.4 0.3 and.27
  183.8 1.0 copy.106
  184.8 1.3 mul.279
  186.1 3.6 %broadcast_in_dim.28 = bf16[1024,2,1024]{2,1,0:T(2,128)(2,1)} broadcast(bf16[1024,1024]{1,0:T(8,128)(2,1)S(1)} %copy-done.1), dimensions={0,2} | broadcast | bytes 6291456 | tf_op jit(solution)/shard_map/broadcast_in_dim | solution.py:171
  189.7 7.3 %reshape.353 = bf16[2048,1024]{1,0:T(8,128)(2,1)} reshape(bf16[1024,2,1024]{2,1,0:T(2,128)(2,1)} %broadcast_in_dim.28) | data formatting | bytes 8388608 | tf_op jit(solution)/shard_map/reshape | solution.py:171
  197.1 4.7 %fusion.2 = bf16[512,1024]{1,0:T(8,128)(2,1)S(1)} fusion(bf16[2048,1024]{1,0:T(8,128)(2,1)} %reshape.353, s32[2048]{0:T(1024)S(1)} %add_select_fusion), kind=kOutput, calls=%fused_computation.3 | convolution fusion | flops 2149056512 | bytes 5251072 | tf_op jit(solution)/shard_map/dot_general | solution.py:172
  201.7 0.4 reshape.354
  202.2 2.3 convolution_bitcast_fusion.1
  204.5 2.3 convolution_convert_fusion
  206.8 1.1 copy.138
  207.9 4.2 %all-to-all-start.1 = ((bf16[4,128,1,4,256]{4,1,3,2,0:T(8,128)(2,1)}), bf16[4,128,1,4,256]{4,1,3,2,0:T(8,128)(2,1)S(1)}, u32[]{:S(2)}, u32[]{:S(2)}) async-start(bf16[4,128,1,4,256]{4,1,3,2,0:T(8,128)(2,1)} %bitcast.122), calls=%async_computation.4 | async-start | bytes 2097152 | tf_op jit(solution)/shard_map/all_to_all | solution.py:32
  212.1 0.7 reduce-scatter.6.cloned.1.call-update
  212.8 13.9 %all-to-all-done.1 = bf16[4,128,1,4,256]{4,1,3,2,0:T(8,128)(2,1)S(1)} async-done(((bf16[4,128,1,4,256]{4,1,3,2,0:T(8,128)(2,1)}), bf16[4,128,1,4,256]{4,1,3,2,0:T(8,128)(2,1)S(1)}, u32[]{:S(2)}, u32[]{:S(2)}) %all-to-all-start.1) | async-done | bytes 1048608 | tf_op jit(solution)/shard_map/all_to_all | solution.py:32
  226.7 0.2 reduce_sum.140
  226.9 0.9 copy.113
  227.8 12.0 %all-to-all-start.2 = ((bf16[128,1,4,256]{3,2,1,0:T(4,128)(2,1)}), bf16[128,1,4,256]{3,2,1,0:T(4,128)(2,1)S(1)}, u32[]{:S(2)}, u32[]{:S(2)}) async-start(bf16[128,1,4,256]{3,2,1,0:T(4,128)(2,1)} %copy.113), calls=%async_computation.5 | async-start | bytes 524288 | tf_op jit(solution)/shard_map/all_to_all | solution.py:185
  240.0 0.2 convert_reduce_fusion.2
  240.5 33.8 %reduce-scatter.6.cloned.1.call-done = f32[4,8,256]{2,1,0:T(8,128)} async-done(((f32[64,8,256]{2,1,0:T(8,128)}), f32[4,8,256]{2,1,0:T(8,128)}) %reduce-scatter.6.cloned.1.call-update) | async-done | bytes 32784 | tf_op jit(solution)/shard_map/reduce_scatter | solution.py:42
  274.4 0.1 fusion.18
  274.6 36.0 %reduce-scatter.8.cloned.1.call-done = f32[1,8,256]{2,1,0:T(8,128)} async-done(((f32[4,8,256]{2,1,0:T(8,128)}), f32[1,8,256]{2,1,0:T(8,128)}) %reduce-scatter.8.cloned.1.call-update) | async-done | bytes 8208 | tf_op jit(solution)/shard_map/reduce_scatter | solution.py:42
  310.6 1.5 fusion.12
  (68 shorter events, 1.7 us)
Async XLA Ops:
  6.5 12.0 %copy-start = (bf16[8,512,1,128]{3,1,2,0:T(8,128)(2,1)S(1)}, bf16[8,512,1,128]{3,1,2,0:T(8,128)(2,1)}, u32[]{:S(2)}) copy-start(bf16[8,512,1,128]{3,1,2,0:T(8,128)(2,1)} %param.26) | copy-start | bytes 3145732
  6.5 12.5 %copy-start.12 = (bf16[8,512,1,128]{3,1,2,0:T(8,128)(2,1)S(1)}, bf16[8,512,1,128]{3,1,2,0:T(8,128)(2,1)}, u32[]{:S(2)}) copy-start(bf16[8,512,1,128]{3,1,2,0:T(8,128)(2,1)} %param.27) | copy-start | bytes 3145732
  6.5 12.8 %copy-start.2 = (bf16[256,1024]{1,0:T(8,128)(2,1)S(1)}, bf16[256,1024]{1,0:T(8,128)(2,1)}, u32[]{:S(2)}) copy-start(bf16[256,1024]{1,0:T(8,128)(2,1)} %param.37) | copy-start | bytes 1572868
  12.7 12.5 %copy-start.10 = (bf16[1024]{0:T(1024)(128)(2,1)S(1)}, bf16[1024]{0:T(1024)(128)(2,1)}, u32[]{:S(2)}) copy-start(bf16[1024]{0:T(1024)(128)(2,1)} %param.38) | copy-start | bytes 6148
  12.7 17.0 %copy-start.3 = (bf16[8,1024]{1,0:T(8,128)(2,1)S(1)}, bf16[8,1024]{1,0:T(8,128)(2,1)}, u32[]{:S(2)}) copy-start(bf16[8,1024]{1,0:T(8,128)(2,1)} %param.24) | copy-start | bytes 49156
  14.1 16.6 %copy-start.8 = (s32[8,2]{0,1:T(2,128)S(1)}, s32[8,2]{0,1:T(2,128)}, u32[]{:S(2)}) copy-start(s32[8,2]{0,1:T(2,128)} %param.43) | copy-start | bytes 196
  15.4 160.4 %copy-start.4 = (bf16[1024,32]{0,1:T(8,128)(2,1)S(1)}, bf16[1024,32]{0,1:T(8,128)(2,1)}, u32[]{:S(2)}) copy-start(bf16[1024,32]{0,1:T(8,128)(2,1)} %param.40) | copy-start | bytes 196612
  19.4 158.9 %copy-start.5 = (bf16[1024,32]{0,1:T(8,128)(2,1)S(1)}, bf16[1024,32]{0,1:T(8,128)(2,1)}, u32[]{:S(2)}) copy-start(bf16[1024,32]{0,1:T(8,128)(2,1)} %param.41) | copy-start | bytes 196612
  19.4 158.9 %copy-start.7 = (bf16[32,256]{1,0:T(8,128)(2,1)S(1)}, bf16[32,256]{1,0:T(8,128)(2,1)}, u32[]{:S(2)}) copy-start(bf16[32,256]{1,0:T(8,128)(2,1)} %param.42) | copy-start | bytes 49156
  20.2 9.5 %all-to-all-start = ((bf16[4,8,1024]{2,1,0:T(8,128)(2,1)}), bf16[4,8,1024]{2,1,0:T(8,128)(2,1)S(1)}, u32[]{:S(2)}, u32[]{:S(2)}) async-start(bf16[4,8,1024]{2,1,0:T(8,128)(2,1)} %broadcast_in_dim.26), calls=%async_computation | async-start | bytes 131072 | tf_op jit(solution)/shard_map/all_to_all | solution.py:16
  25.2 150.6 %all-gather.3.cloned.1.call-start = ((), (), s32[]{:S(2)}) async-start(), calls=%async_computation.6 | async-start | bytes 2113536 | tf_op jit(solution)/shard_map/all_gather | solution.py:155
  30.6 181.5 %reduce-scatter.4.cloned.1.call-start = ((), (), s32[]{:S(2)}) async-start(), calls=%async_computation.7 | async-start | bytes 1572864 | tf_op jit(solution)/shard_map/reduce_scatter | solution.py:42
  175.8 2.5 copy-start.1
  207.9 32.5 %copy-start.11 = (bf16[1024]{0:T(1024)(128)(2,1)S(1)}, bf16[1024]{0:T(1024)(128)(2,1)}, u32[]{:S(2)}) copy-start(bf16[1024]{0:T(1024)(128)(2,1)} %param.39) | copy-start | bytes 6148
  207.9 32.5 %copy-start.9 = (f32[8,2]{0,1:T(2,128)S(1)}, f32[8,2]{0,1:T(2,128)}, u32[]{:S(2)}) copy-start(f32[8,2]{0,1:T(2,128)} %param.44) | copy-start | bytes 196
  207.9 66.5 %copy-start.6 = (bf16[8,1024]{1,0:T(8,128)(2,1)S(1)}, bf16[8,1024]{1,0:T(8,128)(2,1)}, u32[]{:S(2)}) copy-start(bf16[8,1024]{1,0:T(8,128)(2,1)} %multiply_convert_fusion) | copy-start | bytes 49156
  207.9 18.8 %all-to-all-start.1 = ((bf16[4,128,1,4,256]{4,1,3,2,0:T(8,128)(2,1)}), bf16[4,128,1,4,256]{4,1,3,2,0:T(8,128)(2,1)S(1)}, u32[]{:S(2)}, u32[]{:S(2)}) async-start(bf16[4,128,1,4,256]{4,1,3,2,0:T(8,128)(2,1)} %bitcast.122), calls=%async_computation.4 | async-start | bytes 2097152 | tf_op jit(solution)/shard_map/all_to_all | solution.py:32
  212.1 62.3 %reduce-scatter.6.cloned.1.call-start = ((), (), s32[]{:S(2)}) async-start(), calls=%async_computation.8 | async-start | bytes 557056 | tf_op jit(solution)/shard_map/reduce_scatter | solution.py:42
  227.8 46.7 %all-to-all-start.2 = ((bf16[128,1,4,256]{3,2,1,0:T(4,128)(2,1)}), bf16[128,1,4,256]{3,2,1,0:T(4,128)(2,1)S(1)}, u32[]{:S(2)}, u32[]{:S(2)}) async-start(bf16[128,1,4,256]{3,2,1,0:T(4,128)(2,1)} %copy.113), calls=%async_computation.5 | async-start | bytes 524288 | tf_op jit(solution)/shard_map/all_to_all | solution.py:185
  239.8 70.8 %reduce-scatter.8.cloned.1.call-start = ((), (), s32[]{:S(2)}) async-start(), calls=%async_computation.9 | async-start | bytes 40960 | tf_op jit(solution)/shard_map/reduce_scatter | solution.py:42
Sparse Core Ops, SparseCore 0:
  30.7 145.0 all-gather.2
  182.9 16.1 reduce-scatter.3
  215.7 58.6 reduce-scatter.5
  277.0 33.5 reduce-scatter.7
where the time goes:
time: 321 us; the launch traced here: 319 us
  waiting for transfers between devices  143 us (45%)
  blocking collectives  91.3 us (28%)
  matrix products  21.2 us (7%)
  starting transfers between devices  21.2 us (7%)
  local copies, waits for them, and re-layouts  20.5 us (6%)
  between operations  14 us (4%)
  other arithmetic  7.9 us (2%)
    all_gather x1, blocking collectives, per_device(): lax.all_gather(routes, EP, axis=0, tiled=True)  91.3 us
    reduce_scatter x3, waiting for transfers between devices, sum_in_order(): tiles = lax.psum_scatter(tiles, axes[k], scatter_dimension=0, tiled=True)  69.8 us
    all_gather x1, waiting for transfers between devices, per_device(): lax.all_gather(ffn_in, EP, axis=0, tiled=True)  53.6 us
    all_to_all x1, waiting for transfers between devices, summed_on_arrival(): tiles = lax.all_to_all(cut_along(shard, dim, peers), axis, 0, 0, tiled=True)  13.9 us
    all_to_all x1, starting transfers between devices, per_device(): lax.all_to_all(results, EP, split_axis=0, concat_axis=0, tiled=True)  12 us
    reshape x1, local copies, waits for them, and re-layouts, per_device(): repeated_all = jnp.repeat(gathered_rows, topk, axis=0)  7.34 us
  transfers between devices with their start and end apart: 7, of which 5 were waited for; matrix products, arithmetic and copies ran while one was open for 9% of the time, Pallas kernels for 0%

commit v1 on v0

v1 whole, which is shorter than its diff:
```python
import functools

import jax
import jax.numpy as jnp
from jax import lax
from jax.experimental import pallas as pl
from jax.experimental.pallas import tpu as pltpu
from jax.sharding import Mesh
from jax.sharding import PartitionSpec as P

MESH = pl.DeviceIdType.MESH
EP = ("z", "x", "c")
EPS = 1e-06
META = 128
BF = jnp.bfloat16
F32 = jnp.float32


def rms(values, gain):
    return values * lax.rsqrt(jnp.mean(values * values, axis=-1, keepdims=True) + EPS) * gain


def row_of(ref):
    return ref[...].astype(F32).reshape(1, -1)


def nt(a, b):
    return lax.dot_general(a, b, (((1,), (1,)), ((), ())), preferred_element_type=F32)


def mm(a, b):
    return jnp.dot(a, b, preferred_element_type=F32)


def silu(v):
    return v / (1.0 + jnp.exp(-v))


def hi_lo(v):
    hi = v.astype(BF).astype(F32)
    return hi, (v - hi).astype(BF).astype(F32)


def kernel(
    dims,
    tokens, lengths, cum, norm_gain, forget_w, forget_b, query_gain, key_gain, ffn_gain, mix_w,
    routes, route_w,
    keys_h, values_h, qw_h, kw_h, vw_h, ow_h, sg_h, su_h, sd_h, eg_h, eu_h, ed_h,
    out,
    keys, values, wqkv, ow, sg, su, wsd, wgu, wd,
    pt, zb, g, p3, rx1, s1, rx2, zs, rx3, ys, rx4,
    lsem, wsend, wrecv, fsend, frecv, tsend, trecv, zsend, zrecv, xsend, xrecv, csend, crecv,
    c2send, c2recv, x2send, x2recv, z2send, z2recv, ysend, yrecv,
):
    nz, nx, nc, nt_ = dims
    z, x, c, t = (lax.axis_index(a) for a in ("z", "x", "c", "t"))
    batch, depth = tokens.shape
    rows = batch // nt_
    head = keys.shape[2]
    cache = keys.shape[1]
    groups = qw_h.shape[1] // head
    width = depth // nt_
    hidden = eg_h.shape[1]
    strip = nz * rows

    def at(axis, base, step, size):
        return {axis: lax.rem(base + (step % size), size)}

    def idx(base, step, size):
        return lax.rem(base + (step % size), size)

    def rcopy(src, dst, ss, rs, dev):
        return pltpu.make_async_remote_copy(
            src_ref=src, dst_ref=dst, send_sem=ss, recv_sem=rs, device_id=dev, device_id_type=MESH
        )

    barrier = pltpu.get_barrier_semaphore()
    partners = (
        [at("t", t, d, nt_) for d in range(1, nt_)]
        + [at("c", c, d, nc) for d in range(1, nc)]
        + [at("x", x, d, nx) for d in range(1, nx)]
        + [at("z", z, d, nz) for d in range(1, nz)]
    )
    for dev in partners:
        pl.semaphore_signal(barrier, inc=1, device_id=dev, device_id_type=MESH)

    def local(i, src, dst):
        return pltpu.make_async_copy(src, dst, lsem.at[i])

    nq, nk = qw_h.shape[1], kw_h.shape[1]
    loads = [
        local(0, qw_h, wqkv.at[:, 0:nq]),
        local(1, kw_h, wqkv.at[:, nq : nq + nk]),
        local(2, vw_h, wqkv.at[:, nq + nk : nq + 2 * nk]),
        local(3, keys_h, keys),
        local(4, values_h, values),
        local(5, ow_h, ow),
        local(6, eg_h, wgu.at[t, :, 0:hidden]),
        local(7, eu_h, wgu.at[t, :, hidden : 2 * hidden]),
        local(8, ed_h, wd.at[t]),
        local(9, sd_h, wsd.at[t]),
        local(10, sg_h, sg),
        local(11, su_h, su),
    ]
    for cp in loads:
        cp.start()

    tok = tokens[...].astype(F32)
    normed = rms(tok, row_of(norm_gain)).astype(BF)
    logit = jnp.sum(normed.astype(F32) * forget_w[...].astype(F32), axis=-1, keepdims=True) + forget_b[0]
    new_log = jnp.minimum(logit, 0.0) - jnp.log(1.0 + jnp.exp(-jnp.abs(logit)))
    for i in (0, 1, 2):
        loads[i].wait()
    qkv = mm(normed, wqkv[...])
    qg, kg = row_of(query_gain), row_of(key_gain)
    q16 = jnp.concatenate(
        [rms(qkv[:, i * head : (i + 1) * head], qg).astype(BF) for i in range(groups)], axis=0
    )
    new_key = rms(qkv[:, nq : nq + nk], kg).astype(BF).astype(F32)
    new_value = qkv[:, nq + nk : nq + 2 * nk].astype(BF).astype(F32)
    new_key = jnp.concatenate([new_key] * groups, axis=0)
    new_value = jnp.concatenate([new_value] * groups, axis=0)

    n16 = batch * groups
    row16 = lax.rem(lax.broadcasted_iota(jnp.int32, (n16, cache), 0), batch)
    row8 = lax.broadcasted_iota(jnp.int32, (batch, cache), 0)
    pos8 = lax.broadcasted_iota(jnp.int32, (batch, cache), 1)
    length8 = jnp.zeros((batch, cache), jnp.int32)
    cum8 = jnp.zeros((batch, cache), F32)
    for s in range(batch):
        length8 = jnp.where(row8 == s, lengths[s], length8)
        cum8 = jnp.where(row8 == s, cum[s], cum8)
    last = jnp.sum(jnp.where(pos8 == length8 - 1, cum8, 0.0), axis=-1, keepdims=True)
    bias8 = last - cum8 + new_log
    bias8 = jnp.where(pos8 < length8, bias8, -jnp.inf)
    bias16 = jnp.concatenate([bias8] * groups, axis=0)
    loads[3].wait()
    scores = jnp.zeros((n16, cache), F32)
    for s in range(batch):
        scores = jnp.where(row16 == s, nt(q16, keys[s]), scores)
    scale = head ** (-0.5)
    past = jnp.exp(scores * scale + bias16)
    own = jnp.exp(jnp.sum(q16.astype(F32) * new_key, axis=-1, keepdims=True) * scale)
    denominator = jnp.sum(past, axis=-1, keepdims=True) + own
    prob = (past / denominator).astype(BF).astype(F32)
    own_prob = (own / denominator).astype(BF).astype(F32)
    loads[4].wait()
    mixed = own_prob * new_value
    for s in range(batch):
        mixed = mixed + mm(jnp.where(row16 == s, prob, 0.0).astype(BF), values[s])
    mixed = mixed.astype(BF)
    heads = jnp.concatenate([mixed[i * batch : (i + 1) * batch] for i in range(groups)], axis=1)
    loads[5].wait()
    partial = mm(heads, ow[...]).astype(BF)
    pt[t] = partial

    pl.semaphore_wait(barrier, len(partners))
    tsends = []
    for d in range(1, nt_):
        cp = rcopy(pt.at[t], pt.at[t], tsend.at[d], trecv.at[d], at("t", t, d, nt_))
        cp.start()
        tsends.append(cp)

    for i in (6, 7, 8, 9):
        loads[i].wait()
    half = depth // 2
    hhalf = ed_h.shape[0] // 2
    wsends = []
    for k, d in enumerate((1, nt_ - 1)):
        cps = [
            rcopy(wgu.at[t], wgu.at[t], wsend.at[k, 0], wrecv.at[k, 0], at("t", t, d, nt_)),
            rcopy(wd.at[t], wd.at[t], wsend.at[k, 1], wrecv.at[k, 1], at("t", t, d, nt_)),
            rcopy(wsd.at[t], wsd.at[t], wsend.at[k, 2], wrecv.at[k, 2], at("t", t, d, nt_)),
        ]
        for cp in cps:
            cp.start()
        wsends.append(cps)

    rowm = lax.broadcasted_iota(jnp.int32, (batch, META), 0)
    lane = lax.broadcasted_iota(jnp.int32, (batch, META), 1)
    zero = jnp.zeros((batch, META), F32)
    r0, r1, w0, w1 = zero, zero, zero, zero
    for s in range(batch):
        here = rowm == s
        r0 = jnp.where(here, routes[0, s].astype(F32), r0)
        r1 = jnp.where(here, routes[1, s].astype(F32), r1)
        w0 = jnp.where(here, route_w[0, s], w0)
        w1 = jnp.where(here, route_w[1, s], w1)
    total = w0 + w1
    h0, l0 = hi_lo(w0 / total)
    h1, l1 = hi_lo(w1 / total)

    residual = tok + pt[t].astype(F32)
    for d in range(1, nt_):
        peer = idx(t, nt_ - d, nt_)
        rcopy(pt.at[peer], pt.at[peer], tsend.at[d], trecv.at[d], at("t", t, d, nt_)).wait_recv()
        residual = residual + pt[peer].astype(F32)
    ffn = rms(residual, row_of(ffn_gain)).astype(BF).astype(F32)
    gate = jnp.sum(ffn * row_of(mix_w), axis=-1, keepdims=True)
    gate = 1.0 / (1.0 + jnp.exp(-gate))
    hg, lg = hi_lo(jnp.broadcast_to(gate, (batch, META)))
    meta = zero
    for i, v in enumerate((r0, r1, h0, l0, h1, l1, hg, lg)):
        meta = jnp.where(lane == i, v, meta)
    full = jnp.concatenate([ffn, meta], axis=1)

    def own_rows(v):
        sel = v[0:rows]
        for k in range(1, nt_):
            sel = jnp.where(t == k, v[k * rows : (k + 1) * rows], sel)
        return sel

    zb[z] = own_rows(full).astype(BF)
    zsends = []
    for d in sorted(range(1, nz), key=lambda d: -min(d, nz - d)):
        cp = rcopy(zb.at[z], zb.at[z], zsend.at[d], zrecv.at[d], at("z", z, d, nz))
        cp.start()
        zsends.append(cp)

    fsends = []

    def from_neighbour(k, part, ref, peer):
        rcopy(ref.at[peer], ref.at[peer], wsend.at[k, part], wrecv.at[k, part], at("t", t, 1, nt_)).wait_recv()

    left, right = idx(t, nt_ - 1, nt_), idx(t, 1, nt_)
    for d in range(1, nz):
        peer = idx(z, nz - d, nz)
        rcopy(zb.at[peer], zb.at[peer], zsend.at[d], zrecv.at[d], at("z", z, d, nz)).wait_recv()
    g[c, x] = zb[...].reshape(strip, depth + META)

    xsends = []
    for d in range(1, nx):
        cp = rcopy(g.at[c, x], g.at[c, x], xsend.at[d], xrecv.at[d], at("x", x, d, nx))
        cp.start()
        xsends.append(cp)
    twin = {"c": 1 - c}
    cp = rcopy(g.at[c, x], g.at[c, x], csend.at[0], crecv.at[0], twin)
    cp.start()
    xsends.append(cp)

    from_neighbour(0, 0, wgu, left)
    from_neighbour(1, 0, wgu, right)
    fsends += [
        rcopy(wgu.at[left, 0:half], wgu.at[left, 0:half], fsend.at[0, 0], frecv.at[0, 0], at("t", t, 1, nt_)),
        rcopy(wgu.at[right, half:depth], wgu.at[right, half:depth], fsend.at[1, 0], frecv.at[1, 0], at("t", t, nt_ - 1, nt_)),
    ]
    for cp in fsends:
        cp.start()

    for d in range(1, nx):
        peer = idx(x, nx - d, nx)
        rcopy(g.at[c, peer], g.at[c, peer], xsend.at[d], xrecv.at[d], at("x", x, d, nx)).wait_recv()
        cp = rcopy(g.at[c, peer], g.at[c, peer], csend.at[d], crecv.at[d], twin)
        cp.start()
        xsends.append(cp)
    for d in range(nx):
        peer = idx(x, nx - d, nx)
        rcopy(g.at[1 - c, peer], g.at[1 - c, peer], csend.at[d], crecv.at[d], twin).wait_recv()

    from_neighbour(0, 1, wd, left)
    from_neighbour(1, 1, wd, right)
    from_neighbour(0, 2, wsd, left)
    from_neighbour(1, 2, wsd, right)
    more = [
        rcopy(wd.at[left, 0:hhalf], wd.at[left, 0:hhalf], fsend.at[0, 1], frecv.at[0, 1], at("t", t, 1, nt_)),
        rcopy(wd.at[right, hhalf : 2 * hhalf], wd.at[right, hhalf : 2 * hhalf], fsend.at[1, 1], frecv.at[1, 1], at("t", t, nt_ - 1, nt_)),
        rcopy(wsd.at[left], wsd.at[left], fsend.at[0, 2], frecv.at[0, 2], at("t", t, 1, nt_)),
    ]
    for cp in more:
        cp.start()
    fsends += more

    total_rows = nc * nx * strip
    every = g[...].reshape(total_rows, depth + META)
    xs = every[:, 0:depth]
    info = every[:, depth : depth + META].astype(F32)
    mine = ((z * nx + x) * nc + c).astype(F32)
    w = jnp.where(info[:, 0:1] == mine, info[:, 2:3] + info[:, 3:4], 0.0)
    w = w + jnp.where(info[:, 1:2] == mine, info[:, 4:5] + info[:, 5:6], 0.0)
    mg = info[:, 6:7] + info[:, 7:8]

    loads[10].wait()
    loads[11].wait()
    sh = (silu(nt(xs, sg[...])) * nt(xs, su[...])).astype(BF)

    opp = idx(t, 2, nt_)
    hid = []
    for order in range(nt_):
        slot = idx(t, (0, 3, 1, 2)[order], nt_)
        if order == nt_ - 1:
            rcopy(wgu.at[opp, 0:half], wgu.at[opp, 0:half], fsend.at[0, 0], frecv.at[0, 0], at("t", t, 1, nt_)).wait_recv()
            rcopy(wgu.at[opp, half:depth], wgu.at[opp, half:depth], fsend.at[1, 0], frecv.at[1, 0], at("t", t, 1, nt_)).wait_recv()
        pre = mm(xs, wgu[slot])
        hid.append((silu(pre[:, 0:hidden]) * pre[:, hidden : 2 * hidden]).astype(BF))
    rcopy(wd.at[opp, 0:hhalf], wd.at[opp, 0:hhalf], fsend.at[0, 1], frecv.at[0, 1], at("t", t, 1, nt_)).wait_recv()
    rcopy(wd.at[opp, hhalf : 2 * hhalf], wd.at[opp, hhalf : 2 * hhalf], fsend.at[1, 1], frecv.at[1, 1], at("t", t, 1, nt_)).wait_recv()
    rcopy(wsd.at[opp], wsd.at[opp], fsend.at[0, 2], frecv.at[0, 2], at("t", t, 1, nt_)).wait_recv()
    res = mm(hid[0], wd[t])
    for order in range(1, nt_):
        res = res + mm(hid[order], wd[idx(t, (0, 3, 1, 2)[order], nt_)])
    dense = jnp.concatenate([mm(sh, wsd[k]) for k in range(nt_)], axis=1)
    p3[...] = (w * res + mg * dense).astype(BF).reshape(p3.shape)

    cp = rcopy(p3.at[1 - c], rx1, c2send, c2recv, twin)
    cp.start()
    ends = [cp]
    rcopy(p3.at[1 - c], rx1, c2send, c2recv, twin).wait_recv()
    for d in range(1, nx):
        peer = idx(x, d, nx)
        s1[peer] = (p3[c, peer].astype(F32) + rx1[peer].astype(F32)).astype(BF)
        cp = rcopy(s1.at[peer], rx2.at[d], x2send.at[d], x2recv.at[d], at("x", x, d, nx))
        cp.start()
        ends.append(cp)
    acc = p3[c, x].astype(F32) + rx1[x].astype(F32)
    for d in range(1, nx):
        rcopy(s1.at[x], rx2.at[d], x2send.at[d], x2recv.at[d], at("x", x, d, nx)).wait_recv()
        acc = acc + rx2[d].astype(F32)
    zs[...] = acc.astype(BF).reshape(nz, rows, depth)
    for d in sorted(range(1, nz), key=lambda d: -min(d, nz - d)):
        peer = idx(z, d, nz)
        cp = rcopy(zs.at[peer], rx3.at[d], z2send.at[d], z2recv.at[d], {"z": peer})
        cp.start()
        ends.append(cp)
    fin = zs[z].astype(F32)
    for d in range(1, nz):
        rcopy(zs.at[z], rx3.at[d], z2send.at[d], z2recv.at[d], at("z", z, d, nz)).wait_recv()
        fin = fin + rx3[d].astype(F32)

    spread = jnp.concatenate([fin] * nt_, axis=0)
    rowd = lax.broadcasted_iota(jnp.int32, (batch, depth), 0)
    spread = jnp.where((rowd >= t * rows) & (rowd < (t + 1) * rows), spread, 0.0)
    for k in range(nt_):
        ys[k] = spread[:, k * width : (k + 1) * width]
    for d in range(1, nt_):
        peer = idx(t, d, nt_)
        cp = rcopy(ys.at[peer], rx4.at[d], ysend.at[d], yrecv.at[d], {"t": peer})
        cp.start()
        ends.append(cp)
    result = residual[:, 0:width]
    for k in range(1, nt_):
        result = jnp.where(t == k, residual[:, k * width : (k + 1) * width], result)
    result = result + ys[t]
    for d in range(1, nt_):
        rcopy(ys.at[t], rx4.at[d], ysend.at[d], yrecv.at[d], at("t", t, d, nt_)).wait_recv()
        result = result + rx4[d]
    out[...] = result.astype(BF)

    for cp in tsends + zsends + xsends + fsends + ends + wsends[0] + wsends[1]:
        cp.wait_send()


def per_device(
    dims, tokens, lengths, cache_keys, cache_values, cache_cum, norm_gain, query_weight, key_weight,
    value_weight, forget_weight, forget_bias, query_gain, key_gain, out_weight, ffn_gain, mix_weight,
    shared_gate, shared_up, shared_down, routes, route_weights, expert_gate, expert_up, expert_down,
):
    nz, nx, nc, ny = dims
    batch, depth = tokens.shape
    cache, head = cache_keys.shape[1], cache_keys.shape[3]
    rows = batch // ny
    width = depth // ny
    strip = nz * rows
    hidden = expert_gate.shape[2]
    nq, nk = query_weight.shape[1], key_weight.shape[1]
    fs = shared_gate.shape[1]
    vm = pl.BlockSpec(memory_space=pltpu.VMEM)
    sm = pl.BlockSpec(memory_space=pltpu.SMEM)
    hb = pl.BlockSpec(memory_space=pltpu.HBM)
    dma = pltpu.SemaphoreType.DMA
    scratch = [
        pltpu.VMEM((batch, cache, head), BF),
        pltpu.VMEM((batch, cache, head), BF),
        pltpu.VMEM((depth, nq + 2 * nk), BF),
        pltpu.VMEM((nq, depth), BF),
        pltpu.VMEM((fs, depth), BF),
        pltpu.VMEM((fs, depth), BF),
        pltpu.VMEM((ny, fs, width), BF),
        pltpu.VMEM((ny, depth, 2 * hidden), BF),
        pltpu.VMEM((ny, hidden, depth), BF),
        pltpu.VMEM((ny, batch, depth), BF),
        pltpu.VMEM((nz, rows, depth + META), BF),
        pltpu.VMEM((nc, nx, strip, depth + META), BF),
        pltpu.VMEM((nc, nx, strip, depth), BF),
        pltpu.VMEM((nx, strip, depth), BF),
        pltpu.VMEM((nx, strip, depth), BF),
        pltpu.VMEM((nx, strip, depth), BF),
        pltpu.VMEM((nz, rows, depth), BF),
        pltpu.VMEM((nz, rows, depth), BF),
        pltpu.VMEM((ny, batch, width), F32),
        pltpu.VMEM((ny, batch, width), F32),
        dma((12,)),
        dma((2, 3)), dma((2, 3)), dma((2, 3)), dma((2, 3)),
        dma((ny,)), dma((ny,)), dma((nz,)), dma((nz,)), dma((nx,)), dma((nx,)), dma((nx,)), dma((nx,)),
        dma, dma, dma((nx,)), dma((nx,)), dma((nz,)), dma((nz,)), dma((ny,)), dma((ny,)),
    ]
    return pl.pallas_call(
        functools.partial(kernel, dims),
        out_shape=jax.ShapeDtypeStruct((batch, width), BF),
        in_specs=[vm, sm, vm, vm, vm, sm, vm, vm, vm, vm, sm, sm] + [hb] * 12,
        out_specs=vm,
        scratch_shapes=scratch,
        compiler_params=pltpu.CompilerParams(
            collective_id=0, has_side_effects=True, vmem_limit_bytes=48 * 1024 * 1024
        ),
    )(
        tokens, lengths, cache_cum, norm_gain, forget_weight.T, forget_bias, query_gain, key_gain,
        ffn_gain, mix_weight, routes.T, route_weights.T,
        cache_keys.reshape(batch, cache, head), cache_values.reshape(batch, cache, head),
        query_weight, key_weight, value_weight, out_weight, shared_gate.T, shared_up.T, shared_down,
        expert_gate[0], expert_up[0], expert_down[0],
    )


def solution(mesh):
    ep, ny = mesh.shape["ep"], mesh.shape["tp"]
    nz, nx, nc = (16, 4, 2) if ep == 128 else (ep // 4, 2, 2)
    finer = Mesh(mesh.devices.reshape(nz, nx, nc, ny), ("z", "x", "c", "t"))
    placed = (
        P(EP, None),
        P(EP),
        P(EP, None, "t", None),
        P(EP, None, "t", None),
        P(EP, "t", None),
        P(),
        P(None, "t"),
        P(None, "t"),
        P(None, "t"),
        P(None, "t"),
        P("t"),
        P(),
        P(),
        P("t", None),
        P(),
        P(),
        P(None, EP),
        P(None, EP),
        P(EP, "t"),
        P(EP, None),
        P(EP, None),
        P(EP, None, "t"),
        P(EP, None, "t"),
        P(EP, "t", None),
    )
    return jax.shard_map(
        functools.partial(per_device, (nz, nx, nc, ny)),
        mesh=finer, in_specs=placed, out_specs=P(EP, "t"), check_vma=False,
    )
```

time: 321 us -> 83.6 us (0.26)
  waiting for transfers between devices: 143 us -> 0 us
  blocking collectives: 91.3 us -> 0 us
  Pallas kernels: 0 us -> 63.6 us
  matrix products: 21.2 us -> 0 us
  starting transfers between devices: 21.2 us -> 0 us
  between operations: 14 us -> 0.71 us
  other arithmetic: 7.9 us -> 0 us
    all_gather x1 -> x0, blocking collectives: 91.3 us -> none  [per_device(): lax.all_gather(routes, EP, axis=0, tiled=True)]
    reduce_scatter x3 -> x0, waiting for transfers between devices: 69.8 us -> none  [sum_in_order(): tiles = lax.psum_scatter(tiles, axes[k], scatter_dimension=0, tiled=True)]
    pallas_call x0 -> x1, Pallas kernels: none -> 63.6 us  [per_device(): pl.pallas_call(functools.partial(kernel, dims), out_shape=jax.ShapeDtypeS...]
    all_gather x1 -> x0, waiting for transfers between devices: 53.6 us -> none  [per_device(): lax.all_gather(ffn_in, EP, axis=0, tiled=True)]
    dot_general x14 -> x0, matrix products: 21.2 us -> none  [the longest x1 4.65 us: per_device(): jnp.dot(pick_table, repeated_all, preferred_element_type=jnp.float32)]
    all_to_all x3 -> x0, starting transfers between devices: 21.1 us -> none  [the longest x1 12 us: per_device(): lax.all_to_all(results, EP, split_axis=0, concat_axis=0, tiled=True)]
    all_to_all x3 -> x0, waiting for transfers between devices: 18.4 us -> none  [the longest x1 13.9 us: summed_on_arrival(): tiles = lax.all_to_all(cut_along(shard, dim, peers), axis, 0, 0, tiled=True)]
    unnamed x29 -> x47, local copies, waits for them, and re-layouts: 0.16 us -> 18.4 us
  transfers between devices with their start and end apart: 7 -> 0, of which waited for: 5 -> 0; matrix products, arithmetic and copies ran while one was open for 9% -> 0% of each run, Pallas kernels for 0% -> 0%
where the time goes in v1:
time: 83.6 us; the launch traced here: 82.7 us
  Pallas kernels  63.6 us (76%)
  local copies, waits for them, and re-layouts  18.4 us (22%)
    pallas_call x1, Pallas kernels, per_device(): pl.pallas_call(functools.partial(kernel, dims), out_shape=jax.ShapeDtypeS...  63.6 us
    unnamed x47, local copies, waits for them, and re-layouts  18.4 us

profile of v1, /device:TPU:1, one launch (start us, length us, event | category | flops | bytes accessed | tf_op | source)
XLA Modules:
  0.0 82.7 jit_solution(5450530055954270815)
XLA Ops:
  0.0 0.0 copy-start.11
  0.7 0.0 copy-start.14
  0.7 0.0 copy-start.20
  0.7 0.1 copy-done.11
  0.7 0.6 copy-done.14
  1.4 0.0 copy-done.20
  1.4 0.0 copy-start
  1.4 1.2 %copy-done = bf16[8,512,1,128]{3,1,2,0:T(8,128)(2,1)S(1)} copy-done((bf16[8,512,1,128]{3,1,2,0:T(8,128)(2,1)S(1)}, bf16[8,512,1,128]{3,1,2,0:T(8,128)(2,1)}, u32[]{:S(2)}) %copy-start) | copy-done | bytes 1048600
  2.6 0.0 copy-start.1
  2.6 1.2 %copy-done.1 = bf16[8,512,1,128]{3,1,2,0:T(8,128)(2,1)S(1)} copy-done((bf16[8,512,1,128]{3,1,2,0:T(8,128)(2,1)S(1)}, bf16[8,512,1,128]{3,1,2,0:T(8,128)(2,1)}, u32[]{:S(2)}) %copy-start.1) | copy-done | bytes 1048600
  3.8 0.0 copy-start.2
  3.8 1.0 %copy-done.2 = bf16[1024,256]{1,0:T(8,128)(2,1)S(1)} copy-done((bf16[1024,256]{1,0:T(8,128)(2,1)S(1)}, bf16[1024,256]{1,0:T(8,128)(2,1)}, u32[]{:S(2)}) %copy-start.2) | copy-done | bytes 524312
  4.8 0.0 copy-start.3
  4.8 1.0 %copy-done.3 = bf16[256,1024]{1,0:T(8,128)(2,1)S(1)} copy-done((bf16[256,1024]{1,0:T(8,128)(2,1)S(1)}, bf16[256,1024]{1,0:T(8,128)(2,1)}, u32[]{:S(2)}) %copy-start.3) | copy-done | bytes 524312
  5.9 0.0 copy-start.4
  5.9 0.9 %copy-done.4 = bf16[1024,128]{1,0:T(8,128)(2,1)S(1)} copy-done((bf16[1024,128]{1,0:T(8,128)(2,1)S(1)}, bf16[1024,128]{1,0:T(8,128)(2,1)}, u32[]{:S(2)}) %copy-start.4) | copy-done | bytes 262168
  6.8 0.0 copy-start.5
  6.8 0.9 %copy-done.5 = bf16[1024,128]{1,0:T(8,128)(2,1)S(1)} copy-done((bf16[1024,128]{1,0:T(8,128)(2,1)S(1)}, bf16[1024,128]{1,0:T(8,128)(2,1)}, u32[]{:S(2)}) %copy-start.5) | copy-done | bytes 262168
  7.8 0.0 copy-start.6
  7.8 0.9 %copy-done.6 = bf16[1,1024,128]{2,1,0:T(8,128)(2,1)S(1)} copy-done((bf16[1,1024,128]{2,1,0:T(8,128)(2,1)S(1)}, bf16[1,1024,128]{2,1,0:T(8,128)(2,1)}, u32[]{:S(2)}) %copy-start.6) | copy-done | bytes 262168
  8.7 0.0 copy-start.7
  8.7 0.9 %copy-done.7 = bf16[1,1024,128]{2,1,0:T(8,128)(2,1)S(1)} copy-done((bf16[1,1024,128]{2,1,0:T(8,128)(2,1)S(1)}, bf16[1,1024,128]{2,1,0:T(8,128)(2,1)}, u32[]{:S(2)}) %copy-start.7) | copy-done | bytes 262168
  9.7 0.0 copy-start.8
  9.7 0.9 %copy-done.8 = bf16[1,128,1024]{2,1,0:T(8,128)(2,1)S(1)} copy-done((bf16[1,128,1024]{2,1,0:T(8,128)(2,1)S(1)}, bf16[1,128,1024]{2,1,0:T(8,128)(2,1)}, u32[]{:S(2)}) %copy-start.8) | copy-done | bytes 262168
  10.6 0.0 copy-start.9
  10.6 0.8 %copy-done.9 = bf16[1024,32]{0,1:T(8,128)(2,1)S(1)} copy-done((bf16[1024,32]{0,1:T(8,128)(2,1)S(1)}, bf16[1024,32]{0,1:T(8,128)(2,1)}, u32[]{:S(2)}) %copy-start.9) | copy-done | bytes 65560
  11.5 0.0 copy-start.10
  11.5 0.8 %copy-done.10 = bf16[1024,32]{0,1:T(8,128)(2,1)S(1)} copy-done((bf16[1024,32]{0,1:T(8,128)(2,1)S(1)}, bf16[1024,32]{0,1:T(8,128)(2,1)}, u32[]{:S(2)}) %copy-start.10) | copy-done | bytes 65560
  12.3 0.0 copy-start.12
  12.3 0.7 copy-done.12
  13.0 0.0 copy-start.13
  13.0 0.7 copy-done.13
  13.8 0.0 copy-start.15
  13.8 0.7 copy-done.15
  14.4 0.0 copy-start.16
  14.4 0.7 copy-done.16
  15.1 0.0 copy-start.17
  15.1 0.7 copy-done.17
  15.8 0.0 copy-start.18
  15.8 0.7 copy-done.18
  16.5 0.0 copy-start.19
  16.5 0.7 copy-done.19
  17.2 0.0 copy-start.21
  17.2 0.7 copy-done.21
  17.8 0.0 copy-start.22
  17.8 0.7 copy-done.22
  18.5 63.6 %shard_map.226 = bf16[8,256]{1,0:T(8,128)(2,1)S(1)} custom-call(bf16[8,1024]{1,0:T(8,128)(2,1)S(1)} %copy-done.11, s32[8]{0:T(128)S(1)} %copy-done.20, f32[8,1,512]{2,1,0:T(1,128)S(1)} %copy-done.12, bf16[1024]{0:T(1024)(128)(2,1)S(1)} %copy-done.15, bf16[1,1024]{1,0:T(2,128)(2,1)S(1)} %bitcast.17, f32[1]{0:T(128)S(6)} %copy.26.forget_b, ...), custom_call_target="tpu_custom_call" | custom-call | tf_op jit(solution)/shard_map/pallas_call | solution.py:396
  82.1 0.6 copy.27
Async XLA Ops:
  0.0 0.7 copy-start.11
  0.7 0.7 copy-start.14
  0.7 0.7 copy-start.20
  1.4 1.2 %copy-start = (bf16[8,512,1,128]{3,1,2,0:T(8,128)(2,1)S(1)}, bf16[8,512,1,128]{3,1,2,0:T(8,128)(2,1)}, u32[]{:S(2)}) copy-start(bf16[8,512,1,128]{3,1,2,0:T(8,128)(2,1)} %param.26) | copy-start | bytes 3145732
  2.6 1.2 %copy-start.1 = (bf16[8,512,1,128]{3,1,2,0:T(8,128)(2,1)S(1)}, bf16[8,512,1,128]{3,1,2,0:T(8,128)(2,1)}, u32[]{:S(2)}) copy-start(bf16[8,512,1,128]{3,1,2,0:T(8,128)(2,1)} %param.27) | copy-start | bytes 3145732
  3.8 1.0 %copy-start.2 = (bf16[1024,256]{1,0:T(8,128)(2,1)S(1)}, bf16[1024,256]{1,0:T(8,128)(2,1)}, u32[]{:S(2)}) copy-start(bf16[1024,256]{1,0:T(8,128)(2,1)} %qw_h.1) | copy-start | bytes 1572868
  4.8 1.0 %copy-start.3 = (bf16[256,1024]{1,0:T(8,128)(2,1)S(1)}, bf16[256,1024]{1,0:T(8,128)(2,1)}, u32[]{:S(2)}) copy-start(bf16[256,1024]{1,0:T(8,128)(2,1)} %ow_h.1) | copy-start | bytes 1572868
  5.9 0.9 %copy-start.4 = (bf16[1024,128]{1,0:T(8,128)(2,1)S(1)}, bf16[1024,128]{1,0:T(8,128)(2,1)}, u32[]{:S(2)}) copy-start(bf16[1024,128]{1,0:T(8,128)(2,1)} %kw_h.1) | copy-start | bytes 786436
  6.8 0.9 %copy-start.5 = (bf16[1024,128]{1,0:T(8,128)(2,1)S(1)}, bf16[1024,128]{1,0:T(8,128)(2,1)}, u32[]{:S(2)}) copy-start(bf16[1024,128]{1,0:T(8,128)(2,1)} %vw_h.1) | copy-start | bytes 786436
  7.8 0.9 %copy-start.6 = (bf16[1,1024,128]{2,1,0:T(8,128)(2,1)S(1)}, bf16[1,1024,128]{2,1,0:T(8,128)(2,1)}, u32[]{:S(2)}) copy-start(bf16[1,1024,128]{2,1,0:T(8,128)(2,1)} %param.45) | copy-start | bytes 786436
  8.7 0.9 %copy-start.7 = (bf16[1,1024,128]{2,1,0:T(8,128)(2,1)S(1)}, bf16[1,1024,128]{2,1,0:T(8,128)(2,1)}, u32[]{:S(2)}) copy-start(bf16[1,1024,128]{2,1,0:T(8,128)(2,1)} %param.46) | copy-start | bytes 786436
  9.7 0.9 %copy-start.8 = (bf16[1,128,1024]{2,1,0:T(8,128)(2,1)S(1)}, bf16[1,128,1024]{2,1,0:T(8,128)(2,1)}, u32[]{:S(2)}) copy-start(bf16[1,128,1024]{2,1,0:T(8,128)(2,1)} %param.47) | copy-start | bytes 786436
  10.6 0.8 %copy-start.9 = (bf16[1024,32]{0,1:T(8,128)(2,1)S(1)}, bf16[1024,32]{0,1:T(8,128)(2,1)}, u32[]{:S(2)}) copy-start(bf16[1024,32]{0,1:T(8,128)(2,1)} %param.40) | copy-start | bytes 196612
  11.5 0.8 %copy-start.10 = (bf16[1024,32]{0,1:T(8,128)(2,1)S(1)}, bf16[1024,32]{0,1:T(8,128)(2,1)}, u32[]{:S(2)}) copy-start(bf16[1024,32]{0,1:T(8,128)(2,1)} %param.41) | copy-start | bytes 196612
  12.3 0.7 copy-start.12
  13.0 0.7 copy-start.13
  13.8 0.7 copy-start.15
  14.4 0.7 copy-start.16
  15.1 0.7 copy-start.17
  15.8 0.7 copy-start.18
  16.5 0.7 copy-start.19
  17.2 0.7 copy-start.21
  17.8 0.7 copy-start.22
